TPU v7x, 32 devices: a whole 2x2x4 slice. The times are simulated.
32 devices in a mesh: grp: 2 (over y), sp: 4 (over z), tp: 4 (over x, core).
Axes of the slice: x: 2, y: 2, z: 4, core: 2. Of those that a mesh axis runs over, the one named last changes fastest.
Arguments:
- resid_in: bfloat16 [8, 256, 2048], P(('grp', 'tp'), 'sp'), parts along dimension 0, may hold values from -6 to 6
- query_one: bfloat16 [8, 256, 1024], P('grp', 'sp', 'tp'), parts along dimension 0, may hold values from -624 to 624
- key_one: bfloat16 [8, 256, 256], P('grp', 'sp', 'tp'), parts along dimension 0, may hold values from -7.78125 to 7.78125
- query_two: bfloat16 [8, 256, 1024], P('grp', 'sp', 'tp'), parts along dimension 0, may hold values from -624 to 624
- key_two: bfloat16 [8, 256, 256], P('grp', 'sp', 'tp'), parts along dimension 0, may hold values from -7.78125 to 7.78125
- value: bfloat16 [8, 256, 512], P('grp', 'sp', 'tp'), parts along dimension 0, may hold values from -6 to 6
- lam: float32 [32], P('tp'), may hold values from 0.3 to 0.8
- head_gain: float32 [64], replicated, may hold values from 0.1 to 1.9
- doc_ids: int32 [8, 256], P('grp', 'sp'), parts along dimension 0, may hold values from 0 to 3, never falling along the last dimension, each value on 1 to 128 neighbouring positions
- out_weight: bfloat16 [2048, 2048], P('tp'), may hold values from -0.125 to 0.125
- norm_gain: float32 [2048], replicated, may hold values from 0.1 to 1.9
- gate_weight: bfloat16 [2048, 5632], P('sp', 'tp'), may hold values from -0.125 to 0.125
- value_weight: bfloat16 [2048, 5632], P('sp', 'tp'), may hold values from -0.125 to 0.125
- conv_gate: float32 [3, 5632], P(None, 'tp'), may hold values from -3.5 to 3.5
- conv_value: float32 [3, 5632], P(None, 'tp'), may hold values from -3.5 to 3.5
- down_weight: bfloat16 [5632, 2048], P('tp', 'sp'), may hold values from -0.078125 to 0.078125
Outputs:
- resid_out: bfloat16 [8, 256, 2048], P(('grp', 'tp'), 'sp'), parts along dimension 0
There are 2 independent parts, one for each index of `grp`. A program takes and returns all parts, laid end to end along the dimension named above; an argument that names none is the same for every part. Nothing has to cross between parts.
All inputs are finite; a program needn't handle non-finite values.
Results may differ from a plain program's by a relative error of at most 0.014.
Values may be sent and summed in bfloat16 or wider, within the bound.
A program may use at most 128 MiB of HBM per device.

v0:
```python
import math

import jax
import jax.numpy as jnp
from jax import lax
from jax.sharding import PartitionSpec as P

NEG_BIG = -1e30
NORM_EPS = 1e-06
ROPE_BASE = 500000.0


def from_behind(array, axis, by):
    length = lax.axis_size(axis)
    pairs = [(i, i + by) for i in range(length) if 0 <= i + by < length]
    return lax.ppermute(array, axis, pairs)


def rotate(block, positions, heads):
    entries = block.astype(jnp.float32).reshape(block.shape[:-1] + (heads, -1))
    width = entries.shape[-1]
    half = width // 2
    freqs = ROPE_BASE ** (-jnp.arange(half, dtype=jnp.float32) * 2.0 / width)
    angles = positions.astype(jnp.float32)[:, None] * freqs[None, :]
    cosine = jnp.cos(angles)[:, None, :]
    sine = jnp.sin(angles)[:, None, :]
    first = entries[..., :half]
    second = entries[..., half:]
    turned = jnp.concatenate(
        [first * cosine - second * sine, second * cosine + first * sine], axis=-1
    )
    return turned.astype(jnp.bfloat16)


def depthwise(edge, current, taps, edge_docs, docs):
    count = current.shape[0]
    extended = jnp.concatenate([edge, current], axis=0).astype(jnp.float32)
    ext_docs = jnp.concatenate([edge_docs, docs], axis=0)
    total = taps[2][None, :] * extended[2:]
    for shift_k in range(2):
        same = (ext_docs[shift_k : shift_k + count] == docs)[:, None]
        total = total + jnp.where(
            same, taps[shift_k][None, :] * extended[shift_k : shift_k + count], 0.0
        )
    return total


def online_step(state, queries, keys, vals, allowed, scale):
    peak, total, accum = state
    scores = (
        jnp.einsum("sqhgd,skhd->shgqk", queries, keys, preferred_element_type=jnp.float32) * scale
    )
    mask = allowed[:, None, None]
    scores = jnp.where(mask, scores, NEG_BIG)
    new_peak = jnp.maximum(peak, jnp.max(scores, axis=-1))
    expd = jnp.where(mask, jnp.exp(scores - new_peak[..., None]), 0.0)
    fade = jnp.exp(peak - new_peak)
    new_total = total * fade + jnp.sum(expd, axis=-1)
    update = jnp.einsum(
        "shgqk,skhd->shgqd", expd.astype(jnp.bfloat16), vals, preferred_element_type=jnp.float32
    )
    return (new_peak, new_total, accum * fade[..., None] + update)


def per_device(
    resid_in,
    query_one,
    key_one,
    query_two,
    key_two,
    value,
    lam,
    head_gain,
    doc_ids,
    out_weight,
    norm_gain,
    gate_weight,
    value_weight,
    conv_gate,
    conv_value,
    down_weight,
):
    gate_full, value_full, down_full = (
        lax.all_gather(gate_weight, "sp", axis=0, tiled=True),
        lax.all_gather(value_weight, "sp", axis=0, tiled=True),
        lax.all_gather(down_weight, "sp", axis=1, tiled=True),
    )
    seqs = query_one.shape[0]
    rows = query_one.shape[1]
    heads = lam.shape[0]
    key_width = query_one.shape[2] // heads
    kv_local = key_one.shape[2] // key_width
    group = heads // kv_local
    head_width = value.shape[2] // kv_local
    scale = key_width ** (-0.5)
    positions = lax.axis_index("sp") * rows + jnp.arange(rows, dtype=jnp.int32)
    q_first = rotate(query_one, positions, heads).reshape(seqs, rows, kv_local, group, key_width)
    q_second = rotate(query_two, positions, heads).reshape(seqs, rows, kv_local, group, key_width)
    k_first = rotate(key_one, positions, kv_local).reshape(seqs, rows, kv_local * key_width)
    k_second = rotate(key_two, positions, kv_local).reshape(seqs, rows, kv_local * key_width)
    start_state = (
        jnp.full((seqs, kv_local, group, rows), NEG_BIG, jnp.float32),
        jnp.zeros((seqs, kv_local, group, rows), jnp.float32),
        jnp.zeros((seqs, kv_local, group, rows, head_width), jnp.float32),
    )
    keys_one = lax.all_gather(k_first, "sp", axis=1, tiled=True)
    keys_two = lax.all_gather(k_second, "sp", axis=1, tiled=True)
    vals = lax.all_gather(value, "sp", axis=1, tiled=True)
    docs = lax.all_gather(doc_ids, "sp", axis=1, tiled=True)
    count = keys_one.shape[1]
    step_len = math.gcd(count, 512)

    def inner(state, index):
        offset = index * step_len
        ka = lax.dynamic_slice_in_dim(keys_one, offset, step_len, 1).reshape(
            seqs, step_len, kv_local, key_width
        )
        kb = lax.dynamic_slice_in_dim(keys_two, offset, step_len, 1).reshape(
            seqs, step_len, kv_local, key_width
        )
        va = lax.dynamic_slice_in_dim(vals, offset, step_len, 1).reshape(
            seqs, step_len, kv_local, head_width
        )
        dpiece = lax.dynamic_slice_in_dim(docs, offset, step_len, 1)
        key_pos = offset + jnp.arange(step_len, dtype=jnp.int32)
        allowed = (key_pos[None, None, :] <= positions[None, :, None]) & (
            dpiece[:, None, :] == doc_ids[:, :, None]
        )
        first = online_step(state[0], q_first, ka, va, allowed, scale)
        second = online_step(state[1], q_second, kb, va, allowed, scale)
        return ((first, second), None)

    def run(state):
        return lax.scan(inner, state, jnp.arange(count // step_len))[0]

    first, second = lax.cond(
        jnp.int32(0) <= positions[rows - 1], run, lambda state: state, (start_state, start_state)
    )
    weights = lam.reshape(kv_local, group)[None, :, :, None, None]
    mixed = first[2] / first[1][..., None] - weights * (second[2] / second[1][..., None])
    meansq = jnp.mean(mixed * mixed, axis=-1, keepdims=True)
    normed_heads = mixed * lax.rsqrt(meansq + NORM_EPS) * head_gain
    heads_out = jnp.transpose(normed_heads, (0, 3, 1, 2, 4)).reshape(
        seqs * rows, heads * head_width
    )
    heads_out = heads_out.astype(jnp.bfloat16)
    proj = lax.psum_scatter(
        jnp.dot(heads_out, out_weight, preferred_element_type=jnp.float32).astype(jnp.bfloat16),
        "tp",
        scatter_dimension=0,
        tiled=True,
    ).astype(jnp.float32)
    mid = resid_in.astype(jnp.float32) + proj.reshape(resid_in.shape)
    meansq_mid = jnp.mean(mid * mid, axis=-1, keepdims=True)
    normed = (mid * lax.rsqrt(meansq_mid + NORM_EPS) * norm_gain).astype(jnp.bfloat16)
    gathered = lax.all_gather(normed, "tp", axis=0, tiled=True)
    full_rows = gathered.reshape(seqs * rows, gathered.shape[2])
    gate_sum = jnp.dot(full_rows, gate_full, preferred_element_type=jnp.float32)
    value_sum = jnp.dot(full_rows, value_full, preferred_element_type=jnp.float32)
    hidden_width = gate_weight.shape[1]
    up_gate = gate_sum.astype(jnp.bfloat16).reshape(seqs, rows, hidden_width)
    up_value = value_sum.astype(jnp.bfloat16).reshape(seqs, rows, hidden_width)
    tails = jnp.stack([up_gate[:, rows - 2 :], up_value[:, rows - 2 :]], axis=0)
    edges, edge_docs = from_behind((tails, doc_ids[:, rows - 2 :]), "sp", 1)
    sweep = jax.vmap(depthwise, in_axes=(0, 0, None, 0, 0))
    conv_g = sweep(edges[0], up_gate, conv_gate, edge_docs, doc_ids)
    conv_v = sweep(edges[1], up_value, conv_value, edge_docs, doc_ids)
    hidden = (jax.nn.silu(conv_g) * conv_v).astype(jnp.bfloat16).reshape(seqs * rows, hidden_width)
    partial_down = jnp.dot(hidden, down_full, preferred_element_type=jnp.float32)
    down = lax.psum_scatter(
        partial_down.astype(jnp.bfloat16), "tp", scatter_dimension=0, tiled=True
    ).astype(jnp.float32)
    return (mid + down.reshape(mid.shape)).astype(jnp.bfloat16)


def solution(mesh):
    placed = (
        P(("grp", "tp"), "sp", None),
        P("grp", "sp", "tp"),
        P("grp", "sp", "tp"),
        P("grp", "sp", "tp"),
        P("grp", "sp", "tp"),
        P("grp", "sp", "tp"),
        P("tp"),
        P(),
        P("grp", "sp"),
        P("tp", None),
        P(),
        P("sp", "tp"),
        P("sp", "tp"),
        P(None, "tp"),
        P(None, "tp"),
        P("tp", "sp"),
    )
    return jax.shard_map(
        per_device,
        mesh=mesh,
        in_specs=placed,
        out_specs=P(("grp", "tp"), "sp", None),
        check_vma=False,
    )
```

profile of v0, /device:TPU:0, one launch (start us, length us, event | category | flops | bytes accessed | tf_op | source)
XLA Modules:
  0.0 496.4 jit_solution(4319841250001549817)
XLA Ops:
  9.3 1.1 copy.52
  11.8 15.7 %all_gather.25 = bf16[4,256,64]{2,0,1:T(4,128)(2,1)S(1)} all-gather(bf16[4,64,64]{2,0,1:T(4,128)(2,1)S(1)} %copy.47), channel_id=1, replica_groups=mesh['grp'=2,'sp'=4,'tp'=4] {'sp'}, dimensions={1}, use_global_device_ids=true | all-gather | bytes 163840 | tf_op jit(solution)/shard_map/all_gather | solution.py:106
  27.6 15.2 %all_gather.27 = bf16[4,256,64]{2,0,1:T(4,128)(2,1)} all-gather(bf16[4,64,64]{2,0,1:T(4,128)(2,1)S(1)} %copy.51), channel_id=1, replica_groups=mesh['grp'=2,'sp'=4,'tp'=4] {'sp'}, dimensions={1}, use_global_device_ids=true | all-gather | bytes 163840 | tf_op jit(solution)/shard_map/all_gather | solution.py:107
  43.7 15.0 %all_gather.26 = bf16[4,256,128]{2,0,1:T(4,128)(2,1)} all-gather(bf16[4,64,128]{2,0,1:T(4,128)(2,1)S(1)} %copy.49), channel_id=1, replica_groups=mesh['grp'=2,'sp'=4,'tp'=4] {'sp'}, dimensions={1}, use_global_device_ids=true | all-gather | bytes 327680 | tf_op jit(solution)/shard_map/all_gather | solution.py:108
  58.6 12.1 %all-gather = s32[4,64,4]{1,2,0:T(4,128)S(1)} all-gather(s32[1,64,4]{1,2,0:T(4,128)} %bitcast.113), channel_id=1, replica_groups=mesh['grp'=2,'sp'=4,'tp'=4] {'sp'}, dimensions={0}, use_global_device_ids=true | all-gather | bytes 5120 | tf_op jit(solution)/shard_map/all_gather | solution.py:109
  70.8 1.2 slice.86
  72.7 1.3 mul.338
  75.1 13.2 %conditional.1 = (f32[4,2,4,64]{3,2,1,0:T(4,128)S(1)}, f32[4,2,4,64,64]{4,3,2,1,0:T(8,128)S(1)}, f32[4,2,4,64]{3,2,1,0:T(4,128)S(1)}, f32[4,2,4,64,64]{4,3,2,1,0:T(8,128)}) conditional(s32[]{:T(128)} %bitcast.13, () %tuple.15, (s32[64]{0:T(128)S(1)}, s32[4,256]{1,0:T(4,128)S(1)}, s32[4,64]{1,0:T(4,128)S(1)}, bf16[4,256,64]{2,0,1:T(4,128)(2,1)S(1)}, ...), branch_computations={%region_0.0_spmd, %region_1.6_spmd} | conditional | flops 215379968 | bytes 46683620 | solution.py:136
  75.5 2.8 fusion.39
  78.4 2.6 fusion.1
  81.1 1.6 fusion.5
  83.0 3.5 convolution_add_fusion
  86.4 1.8 convolution_add_fusion.1
  88.2 2.1 multiply_reduce_fusion
  91.5 1.7 convolution_convert_fusion
  93.3 24.9 %reduce-scatter.3.cloned.1.call-done = bf16[64,2048]{1,0:T(8,128)(2,1)} async-done(((bf16[256,2048]{1,0:T(8,128)(2,1)}), bf16[64,2048]{1,0:T(8,128)(2,1)}) %reduce-scatter.3.cloned.1.call-update) | async-done | bytes 262160 | tf_op jit(solution)/shard_map/reduce_scatter | solution.py:147
  118.2 1.1 multiply_reduce_fusion.1
  119.4 1.8 multiply_convert_fusion.1
  123.2 3.4 collective-permute-start.1
  126.7 1.2 collective-permute-done.1
  128.0 10.1 %all-gather.6.cloned.1.call-done = bf16[4,64,2048]{2,1,0:T(8,128)(2,1)} async-done(((bf16[1,64,2048]{2,1,0:T(8,128)(2,1)}), bf16[4,64,2048]{2,1,0:T(8,128)(2,1)}) %all-gather.6.cloned.1.call-update) | async-done | bytes 1048592 | tf_op jit(solution)/shard_map/all_gather | solution.py:156
  138.0 108.3 %all-gather.10.cloned.1.call-done = bf16[2048,1408]{1,0:T(8,128)(2,1)} async-done(((bf16[512,1408]{1,0:T(8,128)(2,1)}), bf16[2048,1408]{1,0:T(8,128)(2,1)}) %all-gather.10.cloned.1.call-update) | async-done | bytes 5767184 | tf_op jit(solution)/shard_map/all_gather | solution.py:85
  246.3 4.8 convolution_convert_fusion.1
  251.1 101.6 %all-gather.8.cloned.1.call-done = bf16[2048,1408]{1,0:T(8,128)(2,1)} async-done(((bf16[512,1408]{1,0:T(8,128)(2,1)}), bf16[2048,1408]{1,0:T(8,128)(2,1)}) %all-gather.8.cloned.1.call-update) | async-done | bytes 5767184 | tf_op jit(solution)/shard_map/all_gather | solution.py:84
  352.7 4.8 convolution_convert_fusion.2
  357.6 1.5 collective-permute-start
  359.1 1.4 collective-permute-done
  361.0 1.6 fusion.29
  362.6 96.5 %all-gather.12.cloned.1.call-done = bf16[1408,2048]{1,0:T(8,128)(2,1)} async-done(((bf16[1408,512]{1,0:T(8,128)(2,1)}), bf16[1408,2048]{1,0:T(8,128)(2,1)}) %all-gather.12.cloned.1.call-update) | async-done | bytes 5767184 | tf_op jit(solution)/shard_map/all_gather | solution.py:86
  459.1 5.5 %convolution_convert_fusion.3 = bf16[256,2048]{1,0:T(8,128)(2,1)} fusion(bf16[256,1408]{1,0:T(8,128)(2,1)S(1)} %bitcast.100, bf16[1408,2048]{1,0:T(8,128)(2,1)} %all-gather.12.cloned.1.call-done), kind=kOutput, calls=%fused_computation.39 | convolution fusion | flops 1476919296 | bytes 7536640 | tf_op jit(solution)/shard_map/dot_general | solution.py:169
  464.6 23.2 %reduce-scatter.5.cloned.1.call-done = bf16[64,2048]{1,0:T(8,128)(2,1)} async-done(((bf16[256,2048]{1,0:T(8,128)(2,1)}), bf16[64,2048]{1,0:T(8,128)(2,1)}) %reduce-scatter.5.cloned.1.call-update) | async-done | bytes 262160 | tf_op jit(solution)/shard_map/reduce_scatter | solution.py:170
  487.8 1.7 fusion.37
  (93 shorter events, 10.9 us)
Async XLA Ops:
  6.5 85.0 %copy-start = (bf16[512,2048]{1,0:T(8,128)(2,1)S(1)}, bf16[512,2048]{1,0:T(8,128)(2,1)}, u32[]{:S(2)}) copy-start(bf16[512,2048]{1,0:T(8,128)(2,1)} %param.27) | copy-start | bytes 6291460
  6.5 3.9 copy-start.10
  6.5 4.1 copy-start.11
  6.5 111.7 %reduce-scatter.3.cloned.1.call-start = ((), (), s32[]{:S(2)}) async-start(), calls=%async_computation.2 | async-start | bytes 1310720 | tf_op jit(solution)/shard_map/reduce_scatter | solution.py:147
  27.5 47.5 %copy-start.12 = (s32[4,64]{1,0:T(4,128)S(1)}, s32[4,64]{1,0:T(4,128)}, u32[]{:S(2)}) copy-start(s32[4,64]{1,0:T(4,128)} %param.26) | copy-start | bytes 3076
  27.5 47.5 %copy-start.18 = (s32[64]{0:T(128)S(1)}, s32[64]{0:T(128)}, u32[]{:S(2)}) copy-start(s32[64]{0:T(128)} %iota_add_fusion) | copy-start | bytes 772
  75.1 13.2 %copy-start.16 = (f32[2,4]{1,0:T(2,128)S(1)}, f32[2,4]{1,0:T(2,128)}, u32[]{:S(2)}) copy-start(f32[2,4]{1,0:T(2,128)} %mul.338) | copy-start | bytes 100
  75.1 3.2 copy-start.6
  75.1 3.3 copy-start.8
  78.4 2.6 copy-start.1
  81.0 1.7 copy-start.3
  81.0 1.7 copy-start.7
  82.9 3.5 copy-start.9
  83.0 3.5 copy-start.2
  88.2 2.2 copy-start.17
  91.5 26.7 %copy-start.4 = (bf16[1,64,2048]{2,1,0:T(8,128)(2,1)S(1)}, bf16[1,64,2048]{2,1,0:T(8,128)(2,1)}, u32[]{:S(2)}) copy-start(bf16[1,64,2048]{2,1,0:T(8,128)(2,1)} %param.18) | copy-start | bytes 786436
  91.5 27.9 %copy-start.15 = (f32[2048]{0:T(1024)S(1)}, f32[2048]{0:T(1024)}, u32[]{:S(2)}) copy-start(f32[2048]{0:T(1024)} %param.28) | copy-start | bytes 24580
  93.2 44.8 %all-gather.6.cloned.1.call-start = ((), (), s32[]{:S(2)}) async-start(), calls=%async_computation.3 | async-start | bytes 1310720 | tf_op jit(solution)/shard_map/all_gather | solution.py:156
  121.2 5.4 %copy-start.13 = (f32[3,1408]{1,0:T(4,128)S(1)}, f32[3,1408]{1,0:T(4,128)}, u32[]{:S(2)}) copy-start(f32[3,1408]{1,0:T(4,128)} %param.32) | copy-start | bytes 50692
  121.2 5.4 %copy-start.14 = (f32[3,1408]{1,0:T(4,128)S(1)}, f32[3,1408]{1,0:T(4,128)}, u32[]{:S(2)}) copy-start(f32[3,1408]{1,0:T(4,128)} %param.31) | copy-start | bytes 50692
  121.2 125.1 %all-gather.10.cloned.1.call-start = ((), (), s32[]{:S(2)}) async-start(), calls=%async_computation.5 | async-start | bytes 7208960 | tf_op jit(solution)/shard_map/all_gather | solution.py:85
  121.9 230.8 %all-gather.8.cloned.1.call-start = ((), (), s32[]{:S(2)}) async-start(), calls=%async_computation.4 | async-start | bytes 7208960 | tf_op jit(solution)/shard_map/all_gather | solution.py:84
  122.5 336.6 %all-gather.12.cloned.1.call-start = ((), (), s32[]{:S(2)}) async-start(), calls=%async_computation.6 | async-start | bytes 7208960 | tf_op jit(solution)/shard_map/all_gather | solution.py:86
  123.1 364.7 %reduce-scatter.5.cloned.1.call-start = ((), (), s32[]{:S(2)}) async-start(), calls=%async_computation.7 | async-start | bytes 1310720 | tf_op jit(solution)/shard_map/reduce_scatter | solution.py:170
  123.2 4.7 collective-permute-start.1
  357.6 3.0 collective-permute-start
  459.1 28.7 %copy-start.5 = (bf16[64,2048]{1,0:T(8,128)(2,1)S(1)}, bf16[64,2048]{1,0:T(8,128)(2,1)}, u32[]{:S(2)}) copy-start(bf16[64,2048]{1,0:T(8,128)(2,1)} %reduce-scatter.3.cloned.1.call-done) | copy-start | bytes 786436
Sparse Core Ops, SparseCore 0:
  93.4 24.8 reduce-scatter.2
  121.3 16.6 all-gather.5
  139.6 106.6 all-gather.9
  247.7 104.9 all-gather.7
  354.1 104.9 all-gather.11
  464.7 23.0 reduce-scatter.4
where the time goes:
time: 497 us; the launch traced here: 496 us
  waiting for transfers between devices  369 us (74%)
  blocking collectives  57.9 us (12%)
  matrix products  27.3 us (5%)
  other arithmetic  14.9 us (3%)
  between operations  14.5 us (3%)
  local copies, waits for them, and re-layouts  7.64 us (2%)
  starting transfers between devices  5.04 us (1%)
    all_gather x1, waiting for transfers between devices, per_device(): lax.all_gather(value_weight, 'sp', axis=0, tiled=True)  108 us
    all_gather x1, waiting for transfers between devices, per_device(): lax.all_gather(gate_weight, 'sp', axis=0, tiled=True)  102 us
    all_gather x1, waiting for transfers between devices, per_device(): lax.all_gather(down_weight, 'sp', axis=1, tiled=True)  96.5 us
    reduce_scatter x1, waiting for transfers between devices, per_device(): lax.psum_scatter(jnp.dot(heads_out, out_weight, preferred_element_type=jn...  24.9 us
    reduce_scatter x1, waiting for transfers between devices, per_device(): lax.psum_scatter(partial_down.astype(jnp.bfloat16), 'tp', scatter_dimensi...  23.2 us
    all_gather x1, blocking collectives, per_device(): keys_one = lax.all_gather(k_first, 'sp', axis=1, tiled=True)  15.7 us
    all_gather x1, blocking collectives, per_device(): keys_two = lax.all_gather(k_second, 'sp', axis=1, tiled=True)  15.2 us
    all_gather x1, blocking collectives, per_device(): vals = lax.all_gather(value, 'sp', axis=1, tiled=True)  15 us
  transfers between devices with their start and end apart: 8, of which 8 were waited for; matrix products, arithmetic and copies ran while one was open for 2% of the time, Pallas kernels for 0%

commit v1 on v0

--- a/solution.py
+++ b/solution.py
@@ -8,12 +8,6 @@
 NEG_BIG = -1e30
 NORM_EPS = 1e-06
 ROPE_BASE = 500000.0
-
-
-def from_behind(array, axis, by):
-    length = lax.axis_size(axis)
-    pairs = [(i, i + by) for i in range(length) if 0 <= i + by < length]
-    return lax.ppermute(array, axis, pairs)
 
 
 def rotate(block, positions, heads):
@@ -32,17 +26,50 @@
     return turned.astype(jnp.bfloat16)
 
 
-def depthwise(edge, current, taps, edge_docs, docs):
-    count = current.shape[0]
-    extended = jnp.concatenate([edge, current], axis=0).astype(jnp.float32)
-    ext_docs = jnp.concatenate([edge_docs, docs], axis=0)
-    total = taps[2][None, :] * extended[2:]
-    for shift_k in range(2):
-        same = (ext_docs[shift_k : shift_k + count] == docs)[:, None]
-        total = total + jnp.where(
-            same, taps[shift_k][None, :] * extended[shift_k : shift_k + count], 0.0
-        )
+def depthwise(current, taps, docs):
+    shown = current.astype(jnp.float32)
+    total = taps[2] * shown
+    for back in (1, 2):
+        moved = jnp.pad(shown, ((0, 0), (back, 0), (0, 0)))[:, : shown.shape[1]]
+        moved_docs = jnp.pad(docs, ((0, 0), (back, 0)), constant_values=-1)[:, : docs.shape[1]]
+        total = total + jnp.where((moved_docs == docs)[..., None], taps[2 - back] * moved, 0.0)
     return total
+
+
+def cyclic(array, axis, by):
+    length = lax.axis_size(axis)
+    return lax.ppermute(array, axis, [(i, (i + by) % length) for i in range(length)])
+
+
+def exchange(pieces):
+    count = lax.axis_size("sp")
+    copies = lax.axis_size("grp")
+    me = lax.axis_index("sp")
+    mine = lax.axis_index("grp")
+    if count > 8:
+        return lax.all_to_all(pieces, "sp", 0, 0)
+    shared = pieces.reshape(count, copies, pieces.shape[1] // copies, *pieces.shape[2:])
+    by_shift = [lax.dynamic_index_in_dim(pieces, me, 0, keepdims=False)]
+    for shift in range(1, count):
+        dest = lax.rem(me + shift, count)
+        part = lax.dynamic_slice(
+            shared, (dest, mine) + (0,) * (shared.ndim - 2), (1, 1) + shared.shape[2:]
+        )[0, 0]
+        got = [cyclic(part, "sp", shift)]
+        for turn in range(1, copies):
+            got.append(cyclic(got[0], "grp", turn))
+        got = jnp.stack(got, axis=0)
+        order = [lax.rem(mine - share + copies, copies) for share in range(copies)]
+        got = jnp.stack([lax.dynamic_index_in_dim(got, at, 0, keepdims=False) for at in order])
+        by_shift.append(got.reshape(pieces.shape[1:]))
+    stacked = jnp.stack(by_shift, axis=0)
+    return jnp.stack(
+        [
+            lax.dynamic_index_in_dim(stacked, lax.rem(me - source + count, count), 0, keepdims=False)
+            for source in range(count)
+        ],
+        axis=0,
+    )
 
 
 def online_step(state, queries, keys, vals, allowed, scale):
@@ -80,11 +107,15 @@
     conv_value,
     down_weight,
 ):
-    gate_full, value_full, down_full = (
-        lax.all_gather(gate_weight, "sp", axis=0, tiled=True),
-        lax.all_gather(value_weight, "sp", axis=0, tiled=True),
-        lax.all_gather(down_weight, "sp", axis=1, tiled=True),
-    )
+    n_sp = lax.axis_size("sp")
+    me = lax.axis_index("sp")
+    depth, width = gate_weight.shape
+    share = width // n_sp
+    up_pieces = jnp.stack([gate_weight, value_weight], axis=1).reshape(depth, 2, n_sp, share)
+    up_all = exchange(jnp.transpose(up_pieces, (2, 0, 1, 3)))
+    down_all = exchange(down_weight.reshape(n_sp, share, down_weight.shape[1]))
+    up_all = up_all.reshape(n_sp * depth, 2, share)
+    down_full = jnp.transpose(down_all, (1, 0, 2)).reshape(share, -1)
     seqs = query_one.shape[0]
     rows = query_one.shape[1]
     heads = lam.shape[0]
@@ -103,10 +134,15 @@
         jnp.zeros((seqs, kv_local, group, rows), jnp.float32),
         jnp.zeros((seqs, kv_local, group, rows, head_width), jnp.float32),
     )
-    keys_one = lax.all_gather(k_first, "sp", axis=1, tiled=True)
-    keys_two = lax.all_gather(k_second, "sp", axis=1, tiled=True)
-    vals = lax.all_gather(value, "sp", axis=1, tiled=True)
-    docs = lax.all_gather(doc_ids, "sp", axis=1, tiled=True)
+    packed = jnp.concatenate(
+        [k_first, k_second, value, doc_ids.astype(jnp.bfloat16)[..., None]], axis=-1
+    )
+    packed = lax.all_gather(packed, "sp", axis=1, tiled=True)
+    key_cols = k_first.shape[2]
+    keys_one = packed[..., :key_cols]
+    keys_two = packed[..., key_cols : 2 * key_cols]
+    vals = packed[..., 2 * key_cols : -1]
+    docs = packed[..., -1].astype(jnp.int32)
     count = keys_one.shape[1]
     step_len = math.gcd(count, 512)
 
@@ -153,22 +189,27 @@
     mid = resid_in.astype(jnp.float32) + proj.reshape(resid_in.shape)
     meansq_mid = jnp.mean(mid * mid, axis=-1, keepdims=True)
     normed = (mid * lax.rsqrt(meansq_mid + NORM_EPS) * norm_gain).astype(jnp.bfloat16)
-    gathered = lax.all_gather(normed, "tp", axis=0, tiled=True)
-    full_rows = gathered.reshape(seqs * rows, gathered.shape[2])
-    gate_sum = jnp.dot(full_rows, gate_full, preferred_element_type=jnp.float32)
-    value_sum = jnp.dot(full_rows, value_full, preferred_element_type=jnp.float32)
-    hidden_width = gate_weight.shape[1]
-    up_gate = gate_sum.astype(jnp.bfloat16).reshape(seqs, rows, hidden_width)
-    up_value = value_sum.astype(jnp.bfloat16).reshape(seqs, rows, hidden_width)
-    tails = jnp.stack([up_gate[:, rows - 2 :], up_value[:, rows - 2 :]], axis=0)
-    edges, edge_docs = from_behind((tails, doc_ids[:, rows - 2 :]), "sp", 1)
-    sweep = jax.vmap(depthwise, in_axes=(0, 0, None, 0, 0))
-    conv_g = sweep(edges[0], up_gate, conv_gate, edge_docs, doc_ids)
-    conv_v = sweep(edges[1], up_value, conv_value, edge_docs, doc_ids)
-    hidden = (jax.nn.silu(conv_g) * conv_v).astype(jnp.bfloat16).reshape(seqs * rows, hidden_width)
+    own = normed.shape[0]
+    features = normed.shape[2]
+    gathered = lax.all_gather(normed, ("tp", "sp"), axis=0)
+    gathered = gathered.reshape(-1, n_sp, own, rows, features)
+    full_rows = jnp.transpose(gathered, (0, 2, 1, 3, 4)).reshape(-1, features)
+    total_rows = n_sp * rows
+    start = me * share
+    taps_gate = lax.dynamic_slice_in_dim(conv_gate, start, share, 1)
+    taps_value = lax.dynamic_slice_in_dim(conv_value, start, share, 1)
+    up_gate = jnp.dot(full_rows, up_all[:, 0], preferred_element_type=jnp.float32)
+    up_value = jnp.dot(full_rows, up_all[:, 1], preferred_element_type=jnp.float32)
+    up_gate = up_gate.astype(jnp.bfloat16).reshape(seqs, total_rows, share)
+    up_value = up_value.astype(jnp.bfloat16).reshape(seqs, total_rows, share)
+    conv_g = depthwise(up_gate, taps_gate, docs)
+    conv_v = depthwise(up_value, taps_value, docs)
+    hidden = (jax.nn.silu(conv_g) * conv_v).astype(jnp.bfloat16)
+    hidden = hidden.reshape(-1, own, n_sp, rows, share)
+    hidden = jnp.transpose(hidden, (0, 2, 1, 3, 4)).reshape(-1, share)
     partial_down = jnp.dot(hidden, down_full, preferred_element_type=jnp.float32)
     down = lax.psum_scatter(
-        partial_down.astype(jnp.bfloat16), "tp", scatter_dimension=0, tiled=True
+        partial_down.astype(jnp.bfloat16), ("tp", "sp"), scatter_dimension=0, tiled=True
     ).astype(jnp.float32)
     return (mid + down.reshape(mid.shape)).astype(jnp.bfloat16)
 

time: 497 us -> 292 us (0.59)
  waiting for transfers between devices: 369 us -> 144 us
  blocking collectives: 57.9 us -> 21.3 us
  local copies, waits for them, and re-layouts: 7.64 us -> 40.4 us
  other arithmetic: 14.9 us -> 35 us
  starting transfers between devices: 5.04 us -> 16.3 us
  matrix products: 27.3 us -> 19 us
    all_gather x4 -> x1, waiting for transfers between devices: 317 us -> 0.01 us  [per_device(): gathered = lax.all_gather(normed, ('tp', 'sp'), axis=0)]
    reduce_scatter x1, waiting for transfers between devices: 23.2 us -> 88.7 us  [per_device(): lax.psum_scatter(partial_down.astype(jnp.bfloat16), ('tp', 'sp'), scatter...]
    all_gather x4 -> x1, blocking collectives: 57.9 us -> 21.3 us  [per_device(): packed = lax.all_gather(packed, 'sp', axis=1, tiled=True)]
    ppermute x2 -> x12, waiting for transfers between devices: 2.61 us -> 31.4 us  [cyclic(): lax.ppermute(array, axis, [(i, (i + by) % length) for i in range(length)])]
    ppermute x2 -> x12, starting transfers between devices: 4.84 us -> 16.2 us  [cyclic(): lax.ppermute(array, axis, [(i, (i + by) % length) for i in range(length)])]
    reshape x0 -> x3, local copies, waits for them, and re-layouts: none -> 10.4 us  [the longest x1 6.94 us: exchange(): pieces.reshape(count, copies, pieces.shape[1] // copies, *pieces.shape[2:])]
    another operation x3 -> x14, other arithmetic: 0.25 us -> 10.4 us  [the longest x4 6.15 us: exchange(): got = jnp.stack(got, axis=0)]
    unnamed x30 -> x46, local copies, waits for them, and re-layouts: 3.4 us -> 11.3 us
  transfers between devices with their start and end apart: 8 -> 15, of which waited for: 8 -> 8; matrix products, arithmetic and copies ran while one was open for 2% -> 14% of each run, Pallas kernels for 0% -> 0%
where the time goes in v1:
time: 292 us; the launch traced here: 291 us
  waiting for transfers between devices  144 us (49%)
  local copies, waits for them, and re-layouts  40.4 us (14%)
  other arithmetic  35 us (12%)
  blocking collectives  21.3 us (7%)
  matrix products  19 us (7%)
  starting transfers between devices  16.3 us (6%)
  between operations  14.3 us (5%)
    reduce_scatter x1, waiting for transfers between devices, per_device(): lax.psum_scatter(partial_down.astype(jnp.bfloat16), ('tp', 'sp'), scatter...  88.7 us
    ppermute x12, waiting for transfers between devices, cyclic(): lax.ppermute(array, axis, [(i, (i + by) % length) for i in range(length)])  31.4 us
    reduce_scatter x1, waiting for transfers between devices, per_device(): lax.psum_scatter(jnp.dot(heads_out, out_weight, preferred_element_type=jn...  24.2 us
    all_gather x1, blocking collectives, per_device(): packed = lax.all_gather(packed, 'sp', axis=1, tiled=True)  21.3 us
    ppermute x12, starting transfers between devices, cyclic(): lax.ppermute(array, axis, [(i, (i + by) % length) for i in range(length)])  16.2 us
    unnamed x46, local copies, waits for them, and re-layouts  11.3 us
    reshape x1, local copies, waits for them, and re-layouts, exchange(): pieces.reshape(count, copies, pieces.shape[1] // copies, *pieces.shape[2:])  6.94 us
    another operation x4, other arithmetic, exchange(): got = jnp.stack(got, axis=0)  6.15 us
  transfers between devices with their start and end apart: 15, of which 8 were waited for; matrix products, arithmetic and copies ran while one was open for 14% of the time, Pallas kernels for 0%

profile of v1, /device:TPU:0, one launch (start us, length us, event | category | flops | bytes accessed | tf_op | source)
XLA Modules:
  0.0 290.8 jit_solution(16987725500709630848)
XLA Ops:
  11.4 21.3 %all_gather.9 = bf16[4,256,257]{2,0,1:T(4,128)(2,1)S(1)} all-gather(bf16[4,64,257]{2,0,1:T(4,128)(2,1)S(1)} %pad_maximum_fusion.11), channel_id=1, replica_groups=mesh['grp'=2,'sp'=4,'tp'=4] {'sp'}, dimensions={1}, use_global_device_ids=true | all-gather | bytes 657920 | tf_op jit(solution)/shard_map/all_gather | solution.py:140
  36.3 1.8 convert.49
  42.9 8.3 %conditional.1 = (f32[4,2,4,64]{3,2,1,0:T(4,128)S(1)}, f32[4,2,4,64,64]{4,3,2,1,0:T(8,128)}, f32[4,2,4,64]{3,2,1,0:T(4,128)S(1)}, f32[4,2,4,64,64]{4,3,2,1,0:T(8,128)}) conditional(s32[]{:T(128)} %bitcast.13, () %tuple.15, (s32[64]{0:T(128)S(1)}, s32[4,256]{1,0:T(4,128)S(1)}, s32[4,64]{1,0:T(4,128)S(1)}, bf16[4,256,257]{2,0,1:T(4,128)(2,1)S(1)}, ...), branch_computations={%region_0.1_spmd, %region_1.6_spmd} | conditional | flops 215379968 | bytes 19948860 | solution.py:172
  46.2 1.6 fusion.5
  47.9 1.7 convolution_add_fusion
  49.6 1.6 convolution_add_fusion.1
  51.2 2.3 multiply_reduce_fusion
  54.7 1.7 convolution_convert_fusion.1
  56.4 24.2 %reduce-scatter.3.cloned.1.call-done = bf16[64,2048]{1,0:T(8,128)(2,1)} async-done(((bf16[256,2048]{1,0:T(8,128)(2,1)}), bf16[64,2048]{1,0:T(8,128)(2,1)}) %reduce-scatter.3.cloned.1.call-update) | async-done | bytes 262160 | tf_op jit(solution)/shard_map/reduce_scatter | solution.py:183
  81.8 1.8 multiply_convert_fusion.1
  83.7 1.8 dynamic-slice_bitcast_fusion.2
  85.5 2.4 collective-permute-start.8
  89.9 1.7 copy.115
  91.7 1.7 copy.116
  93.4 1.9 fusion.26
  95.3 6.9 %reshape.250 = bf16[4,2,256,2,352]{2,1,4,0,3:T(2,128)(2,1)} reshape(bf16[4,512,2,352]{1,3,0,2:T(8,128)(2,1)} %fusion.26) | data formatting | bytes 5767168 | tf_op jit(solution)/shard_map/reshape | solution.py:51
  102.2 4.6 %constant_dynamic-slice_fusion.12 = (bf16[1,1,256,2,352]{2,1,4,0,3:T(2,128)(2,1)S(1)}, bf16[1,1,256,2,352]{2,1,4,0,3:T(2,128)(2,1)S(1)}, bf16[1,1,256,2,352]{2,1,4,0,3:T(2,128)(2,1)}) fusion(bf16[4,2,256,2,352]{2,1,4,0,3:T(2,128)(2,1)} %reshape.250, s32[]{:T(128)S(6)} %select_n.95, s32[]{:T(128)S(6)} %select_n.96, s32[]{:T(128)S(6)} %select_n.99, ...), kind=kLoop, calls=%fused_computation.160 | loop fusion | bytes 2162704 | tf_op jit(solution)/shard_map/dynamic_slice | solution.py:55
  109.9 2.3 collective-permute-start.2
  120.6 2.3 collective-permute-done.11
  128.1 16.7 %collective-permute-done.2 = bf16[256,2,352]{0,2,1:T(8,128)(2,1)} collective-permute-done((bf16[256,2,352]{0,2,1:T(8,128)(2,1)}, bf16[256,2,352]{0,2,1:T(8,128)(2,1)}, u32[]{:S(2)}, u32[]{:S(2)}) %collective-permute-start.2) | collective-permute-done | bytes 360480 | tf_op jit(solution)/shard_map/ppermute | solution.py:41
  146.2 9.3 %collective-permute-done.4 = bf16[256,2,352]{0,2,1:T(8,128)(2,1)S(1)} collective-permute-done((bf16[256,2,352]{0,2,1:T(8,128)(2,1)S(1)}, bf16[256,2,352]{0,2,1:T(8,128)(2,1)S(1)}, u32[]{:S(2)}, u32[]{:S(2)}) %collective-permute-start.4) | collective-permute-done | bytes 360480 | tf_op jit(solution)/shard_map/ppermute | solution.py:41
  161.2 1.8 collective-permute-done.5
  163.0 2.4 fusion.52
  168.9 1.6 pad_maximum_fusion.1
  171.1 2.0 copy.132
  173.2 4.5 %fusion.44 = f32[1024,352]{0,1:T(8,128)S(1)} fusion(bf16[1024,2048]{1,0:T(8,128)(2,1)} %bitcast.191, bf16[2048,2,352]{0,2,1:T(8,128)(2,1)} %bitcast.161), kind=kOutput, calls=%fused_computation.70 | convolution fusion | flops 1477115904 | bytes 7077888 | tf_op jit(solution)/shard_map/dot_general | solution.py:201
  177.9 2.8 fusion.46
  181.4 1.9 reshape.269
  183.4 5.9 %fusion.42 = bf16[4,256,352]{1,0,2:T(4,128)(2,1)S(1)} fusion(f32[4,256,352]{1,0,2:T(4,128)S(1)} %reshape.269, f32[4,256,352]{1,0,2:T(4,128)S(1)} %reshape.268, f32[352]{0:T(512)S(1)} %get-tuple-element.108, f32[352]{0:T(512)S(1)} %get-tuple-element.107, f32[352]{0:T(512)S(1)} %get-tuple-element.106, f32[352]{0:T(512)S(1)} %get-tuple-element.170, ...), kind=kLoop, calls=%fused_computation.68 | loop fusion | flops 7208960 | bytes 3614976 | tf_op jit(solution)/shard_map/convert_element_type | solution.py:207
  189.4 4.3 %convolution_convert_fusion = bf16[1024,2048]{1,0:T(8,128)(2,1)} fusion(bf16[1024,352]{0,1:T(8,128)(2,1)S(1)} %bitcast.170, bf16[352,2048]{1,0:T(8,128)(2,1)S(1)} %bitcast.164), kind=kOutput, calls=%fused_computation.36 | convolution fusion | flops 1478492160 | bytes 6356992 | tf_op jit(solution)/shard_map/dot_general | solution.py:210
  193.8 88.7 %reduce-scatter.5.cloned.1.call-done = bf16[64,2048]{1,0:T(8,128)(2,1)} async-done(((bf16[1024,2048]{1,0:T(8,128)(2,1)}), bf16[64,2048]{1,0:T(8,128)(2,1)}) %reduce-scatter.5.cloned.1.call-update) | async-done | bytes 262160 | tf_op jit(solution)/shard_map/reduce_scatter | solution.py:211
  282.5 1.7 fusion.50
  (133 shorter events, 48.9 us)
Async XLA Ops:
  6.5 48.1 %copy-start = (bf16[512,2048]{1,0:T(8,128)(2,1)S(1)}, bf16[512,2048]{1,0:T(8,128)(2,1)}, u32[]{:S(2)}) copy-start(bf16[512,2048]{1,0:T(8,128)(2,1)} %param.27) | copy-start | bytes 6291460
  6.5 27.1 %copy-start.9 = (bf16[4,64,256]{2,1,0:T(8,128)(2,1)S(1)}, bf16[4,64,256]{2,1,0:T(8,128)(2,1)}, u32[]{:S(2)}) copy-start(bf16[4,64,256]{2,1,0:T(8,128)(2,1)} %param.19) | copy-start | bytes 393220
  6.5 74.1 %reduce-scatter.3.cloned.1.call-start = ((), (), s32[]{:S(2)}) async-start(), calls=%async_computation.2 | async-start | bytes 1310720 | tf_op jit(solution)/shard_map/reduce_scatter | solution.py:183
  9.2 26.3 %copy-start.10 = (bf16[4,64,256]{2,1,0:T(8,128)(2,1)S(1)}, bf16[4,64,256]{2,1,0:T(8,128)(2,1)}, u32[]{:S(2)}) copy-start(bf16[4,64,256]{2,1,0:T(8,128)(2,1)} %param.21) | copy-start | bytes 393220
  36.3 6.5 %copy-start.11 = (s32[4,256]{1,0:T(4,128)S(1)}, s32[4,256]{1,0:T(4,128)}, u32[]{:S(2)}) copy-start(s32[4,256]{1,0:T(4,128)} %bitcast_convert_fusion) | copy-start | bytes 12292
  36.3 6.5 %copy-start.14 = (s32[4,64]{1,0:T(4,128)S(1)}, s32[4,64]{1,0:T(4,128)}, u32[]{:S(2)}) copy-start(s32[4,64]{1,0:T(4,128)} %param.26) | copy-start | bytes 3076
  36.3 6.5 %copy-start.16 = (s32[64]{0:T(128)S(1)}, s32[64]{0:T(128)}, u32[]{:S(2)}) copy-start(s32[64]{0:T(128)} %iota_add_fusion) | copy-start | bytes 772
  51.2 2.3 copy-start.15
  54.6 26.0 %copy-start.3 = (bf16[1,64,2048]{2,1,0:T(8,128)(2,1)S(1)}, bf16[1,64,2048]{2,1,0:T(8,128)(2,1)}, u32[]{:S(2)}) copy-start(bf16[1,64,2048]{2,1,0:T(8,128)(2,1)} %param.18) | copy-start | bytes 786436
  54.6 27.2 %copy-start.13 = (f32[2048]{0:T(1024)S(1)}, f32[2048]{0:T(1024)}, u32[]{:S(2)}) copy-start(f32[2048]{0:T(1024)} %param.28) | copy-start | bytes 24580
  56.4 116.8 %all-gather.3.cloned.1.call-start = ((), (), s32[]{:S(2)}) async-start(), calls=%async_computation.4 | async-start | bytes 4456448 | tf_op jit(solution)/shard_map/all_gather | solution.py:194
  83.6 198.9 %reduce-scatter.5.cloned.1.call-start = ((), (), s32[]{:S(2)}) async-start(), calls=%async_computation.3 | async-start | bytes 4456448 | tf_op jit(solution)/shard_map/reduce_scatter | solution.py:211
  85.5 26.8 %collective-permute-start.8 = (bf16[176,512]{1,0:T(8,128)(2,1)S(1)}, bf16[176,512]{1,0:T(8,128)(2,1)S(1)}, u32[]{:S(2)}, u32[]{:S(2)}) collective-permute-start(bf16[176,512]{1,0:T(8,128)(2,1)S(1)} %get-tuple-element.133), channel_id=1, source_target_pairs={{0,8},{4,12},{8,0},{12,4},{1,9},{5,13},{9,1},{13,5},{2,10},{6,14},... | collective-permute-start | bytes 540680 | tf_op jit(solution)/shard_map/ppermute | solution.py:41
  87.9 25.9 %collective-permute-start.10 = (bf16[176,512]{1,0:T(8,128)(2,1)S(1)}, bf16[176,512]{1,0:T(8,128)(2,1)}, u32[]{:S(2)}, u32[]{:S(2)}) collective-permute-start(bf16[176,512]{1,0:T(8,128)(2,1)S(1)} %get-tuple-element.132), channel_id=1, source_target_pairs={{0,12},{4,0},{8,4},{12,8},{1,13},{5,1},{9,5},{13,9},{2,14},{6,2},{... | collective-permute-start | bytes 540680 | tf_op jit(solution)/shard_map/ppermute | solution.py:41
  89.3 29.2 %collective-permute-start.6 = (bf16[176,512]{1,0:T(8,128)(2,1)}, bf16[176,512]{1,0:T(8,128)(2,1)}, u32[]{:S(2)}, u32[]{:S(2)}) collective-permute-start(bf16[176,512]{1,0:T(8,128)(2,1)} %get-tuple-element.131), channel_id=1, source_target_pairs={{0,4},{4,8},{8,12},{12,0},{1,5},{5,9},{9,13},{13,1},{2,6},{6,10},{... | collective-permute-start | bytes 540680 | tf_op jit(solution)/shard_map/ppermute | solution.py:41
  106.8 5.4 %copy-start.12 = (s32[4,256]{1,0:T(4,128)S(1)}, s32[4,256]{1,0:T(4,128)}, u32[]{:S(2)}) copy-start(s32[4,256]{1,0:T(4,128)} %bitcast_convert_fusion) | copy-start | bytes 12292
  107.7 16.7 %collective-permute-start = (bf16[256,2,352]{0,2,1:T(8,128)(2,1)}, bf16[256,2,352]{0,2,1:T(8,128)(2,1)}, u32[]{:S(2)}, u32[]{:S(2)}) collective-permute-start(bf16[256,2,352]{0,2,1:T(8,128)(2,1)} %bitcast.156), channel_id=1, source_target_pairs={{0,4},{4,8},{8,12},{12,0},{1,5},{5,9},{9,13},{13,1},{2,6},{6,10},{... | collective-permute-start | bytes 1081352 | tf_op jit(solution)/shard_map/ppermute | solution.py:41
  109.9 34.9 %collective-permute-start.2 = (bf16[256,2,352]{0,2,1:T(8,128)(2,1)}, bf16[256,2,352]{0,2,1:T(8,128)(2,1)}, u32[]{:S(2)}, u32[]{:S(2)}) collective-permute-start(bf16[256,2,352]{0,2,1:T(8,128)(2,1)} %bitcast.155), channel_id=1, source_target_pairs={{0,8},{4,12},{8,0},{12,4},{1,9},{5,13},{9,1},{13,5},{2,10},{6,14},... | collective-permute-start | bytes 1081352 | tf_op jit(solution)/shard_map/ppermute | solution.py:41
  112.3 4.2 %copy-start.8 = (bf16[176,512]{1,0:T(8,128)(2,1)}, bf16[176,512]{1,0:T(8,128)(2,1)S(1)}, u32[]{:S(2)}) copy-start(bf16[176,512]{1,0:T(8,128)(2,1)S(1)} %collective-permute-done.8) | copy-start | bytes 540676
  112.3 6.8 %collective-permute-start.9 = (bf16[176,512]{1,0:T(8,128)(2,1)S(1)}, bf16[176,512]{1,0:T(8,128)(2,1)}, u32[]{:S(2)}, u32[]{:S(2)}) collective-permute-start(bf16[176,512]{1,0:T(8,128)(2,1)S(1)} %collective-permute-done.8), channel_id=1, source_target_pairs={{0,16},{16,0},{1,17},{17,1},{2,18},{18,2},{3,19},{19,3},{4,20},{20... | collective-permute-start | bytes 540680 | tf_op jit(solution)/shard_map/ppermute | solution.py:41
  113.8 9.0 %collective-permute-start.11 = (bf16[176,512]{1,0:T(8,128)(2,1)}, bf16[176,512]{1,0:T(8,128)(2,1)}, u32[]{:S(2)}, u32[]{:S(2)}) collective-permute-start(bf16[176,512]{1,0:T(8,128)(2,1)} %collective-permute-done.10), channel_id=1, source_target_pairs={{0,16},{16,0},{1,17},{17,1},{2,18},{18,2},{3,19},{19,3},{4,20},{20... | collective-permute-start | bytes 540680 | tf_op jit(solution)/shard_map/ppermute | solution.py:41
  118.5 36.9 %collective-permute-start.4 = (bf16[256,2,352]{0,2,1:T(8,128)(2,1)S(1)}, bf16[256,2,352]{0,2,1:T(8,128)(2,1)S(1)}, u32[]{:S(2)}, u32[]{:S(2)}) collective-permute-start(bf16[256,2,352]{0,2,1:T(8,128)(2,1)S(1)} %bitcast.179), channel_id=1, source_target_pairs={{0,12},{4,0},{8,4},{12,8},{1,13},{5,1},{9,5},{13,9},{2,14},{6,2},{... | collective-permute-start | bytes 1081352 | tf_op jit(solution)/shard_map/ppermute | solution.py:41
  119.1 7.6 %collective-permute-start.7 = (bf16[176,512]{1,0:T(8,128)(2,1)}, bf16[176,512]{1,0:T(8,128)(2,1)S(1)}, u32[]{:S(2)}, u32[]{:S(2)}) collective-permute-start(bf16[176,512]{1,0:T(8,128)(2,1)} %collective-permute-done.6), channel_id=1, source_target_pairs={{0,16},{16,0},{1,17},{17,1},{2,18},{18,2},{3,19},{19,3},{4,20},{20... | collective-permute-start | bytes 540680 | tf_op jit(solution)/shard_map/ppermute | solution.py:41
  124.4 34.2 %collective-permute-start.1 = (bf16[256,2,352]{0,2,1:T(8,128)(2,1)}, bf16[256,2,352]{0,2,1:T(8,128)(2,1)S(1)}, u32[]{:S(2)}, u32[]{:S(2)}) collective-permute-start(bf16[256,2,352]{0,2,1:T(8,128)(2,1)} %collective-permute-done), channel_id=1, source_target_pairs={{0,16},{16,0},{1,17},{17,1},{2,18},{18,2},{3,19},{19,3},{4,20},{20... | collective-permute-start | bytes 1081352 | tf_op jit(solution)/shard_map/ppermute | solution.py:41
  144.8 16.4 %collective-permute-start.3 = (bf16[256,2,352]{0,2,1:T(8,128)(2,1)}, bf16[256,2,352]{0,2,1:T(8,128)(2,1)S(1)}, u32[]{:S(2)}, u32[]{:S(2)}) collective-permute-start(bf16[256,2,352]{0,2,1:T(8,128)(2,1)} %collective-permute-done.2), channel_id=1, source_target_pairs={{0,16},{16,0},{1,17},{17,1},{2,18},{18,2},{3,19},{19,3},{4,20},{20... | collective-permute-start | bytes 1081352 | tf_op jit(solution)/shard_map/ppermute | solution.py:41
  155.4 7.5 %collective-permute-start.5 = (bf16[256,2,352]{0,2,1:T(8,128)(2,1)S(1)}, bf16[256,2,352]{0,2,1:T(8,128)(2,1)}, u32[]{:S(2)}, u32[]{:S(2)}) collective-permute-start(bf16[256,2,352]{0,2,1:T(8,128)(2,1)S(1)} %collective-permute-done.4), channel_id=1, source_target_pairs={{0,16},{16,0},{1,17},{17,1},{2,18},{18,2},{3,19},{19,3},{4,20},{20... | collective-permute-start | bytes 1081352 | tf_op jit(solution)/shard_map/ppermute | solution.py:41
  173.2 4.5 %copy-start.2 = (bf16[4,2,44,8,512]{4,3,0,2,1:T(8,128)(2,1)S(1)}, bf16[4,2,44,8,512]{4,3,0,2,1:T(8,128)(2,1)}, u32[]{:S(2)}) copy-start(bf16[4,2,44,8,512]{4,3,0,2,1:T(8,128)(2,1)} %copy.132) | copy-start | bytes 8650756
  173.2 4.7 %copy-start.17 = (bf16[16,64,2048]{2,1,0:T(8,128)(2,1)S(1)}, bf16[16,64,2048]{2,1,0:T(8,128)(2,1)}, u32[]{:S(2)}) copy-start(bf16[16,64,2048]{2,1,0:T(8,128)(2,1)} %all-gather.3.cloned.1.call-done) | copy-start | bytes 12582916
  183.3 6.1 %copy-start.6 = (bf16[4,44,8,512]{3,2,0,1:T(8,128)(2,1)S(1)}, bf16[4,44,8,512]{3,2,0,1:T(8,128)(2,1)}, u32[]{:S(2)}) copy-start(bf16[4,44,8,512]{3,2,0,1:T(8,128)(2,1)} %copy.133) | copy-start | bytes 4325380
  193.8 90.5 %copy-start.1 = (bf16[512,2048]{1,0:T(8,128)(2,1)S(1)}, bf16[512,2048]{1,0:T(8,128)(2,1)}, u32[]{:S(2)}) copy-start(bf16[512,2048]{1,0:T(8,128)(2,1)} %param.27) | copy-start | bytes 6291460
  193.8 88.7 %copy-start.4 = (bf16[1,64,2048]{2,1,0:T(8,128)(2,1)S(1)}, bf16[1,64,2048]{2,1,0:T(8,128)(2,1)}, u32[]{:S(2)}) copy-start(bf16[1,64,2048]{2,1,0:T(8,128)(2,1)} %param.18) | copy-start | bytes 786436
  193.8 88.7 %copy-start.5 = (bf16[64,2048]{1,0:T(8,128)(2,1)S(1)}, bf16[64,2048]{1,0:T(8,128)(2,1)}, u32[]{:S(2)}) copy-start(bf16[64,2048]{1,0:T(8,128)(2,1)} %reduce-scatter.3.cloned.1.call-done) | copy-start | bytes 786436
  (1 other events, 1.7 us)
Sparse Core Ops, SparseCore 0:
  56.5 24.1 reduce-scatter.2
  83.7 76.0 all-gather.2
  193.9 88.5 reduce-scatter.4

commit v2 on v1

--- a/solution.py
+++ b/solution.py
@@ -1,13 +1,242 @@
+import functools
 import math
 
 import jax
 import jax.numpy as jnp
 from jax import lax
+from jax.experimental import pallas as pl
+from jax.experimental.pallas import tpu as pltpu
 from jax.sharding import PartitionSpec as P
 
 NEG_BIG = -1e30
 NORM_EPS = 1e-06
 ROPE_BASE = 500000.0
+
+
+MESH = pl.DeviceIdType.MESH
+VMEM = pl.BlockSpec(memory_space=pltpu.VMEM)
+
+
+def greet(devices):
+    barrier = pltpu.get_barrier_semaphore()
+    for device in devices:
+        pl.semaphore_signal(barrier, inc=1, device_id=device, device_id_type=MESH)
+    pl.semaphore_wait(barrier, len(devices))
+
+
+def remote(src, dst, send_sem, recv_sem, device):
+    return pltpu.make_async_remote_copy(
+        src_ref=src,
+        dst_ref=dst,
+        send_sem=send_sem,
+        recv_sem=recv_sem,
+        device_id=device,
+        device_id_type=MESH,
+    )
+
+
+def partners():
+    at = lax.axis_index("tp")
+    return at, at + 1 - 2 * lax.rem(at, 2), lax.rem(at + 2, 4)
+
+
+def spread_kernel(n, own_ref, out_ref, send_sem, recv_sem):
+    me = lax.axis_index("sp")
+    peers = [lax.rem(me + shift, n) for shift in range(1, n)]
+    greet([{"sp": peer} for peer in peers])
+    copies = []
+    for k, peer in enumerate(peers):
+        copy = remote(
+            own_ref, out_ref.at[:, me], send_sem.at[k], recv_sem.at[k], {"sp": peer}
+        )
+        copy.start()
+        copies.append(copy)
+    out_ref[:, me] = own_ref[...]
+    for copy in copies:
+        copy.wait_recv()
+    for copy in copies:
+        copy.wait_send()
+
+
+def gather_sp(own):
+    n = lax.axis_size("sp")
+    if n > 8:
+        return lax.all_gather(own, "sp", axis=1, tiled=True)
+    outer, rows, width = own.shape
+    out = pl.pallas_call(
+        functools.partial(spread_kernel, n),
+        out_shape=jax.ShapeDtypeStruct((outer, n, rows, width), own.dtype),
+        in_specs=[VMEM],
+        out_specs=VMEM,
+        scratch_shapes=[pltpu.SemaphoreType.DMA((n - 1,)), pltpu.SemaphoreType.DMA((n - 1,))],
+        compiler_params=pltpu.CompilerParams(collective_id=1, has_side_effects=True),
+        cost_estimate=pl.CostEstimate(flops=0, bytes_accessed=30_000_000, transcendentals=0),
+        name="gather_sp",
+    )(own)
+    return out.reshape(outer, n * rows, width)
+
+
+def rows_kernel(n, own_ref, out_ref, z_send, z_recv, x_send, x_recv, c_send, c_recv):
+    me = lax.axis_index("sp")
+    tp, near, far = partners()
+    greet([{"tp": near}, {"tp": far}] + [{"sp": lax.rem(me + k, n)} for k in range(1, n)])
+    sources = [lax.rem(me - k + n, n) for k in range(n)]
+    z_copies = []
+    for k in range(1, n):
+        copy = remote(
+            own_ref,
+            out_ref.at[tp, me],
+            z_send.at[k - 1],
+            z_recv.at[k - 1],
+            {"sp": lax.rem(me + k, n)},
+        )
+        z_copies.append(copy)
+
+    def along(owner, k, send, recv, device):
+        block = out_ref.at[owner, sources[k]]
+        return remote(block, block, send, recv, device)
+
+    x_copies = [remote(own_ref, out_ref.at[tp, me], x_send.at[0], x_recv.at[0], {"tp": far})]
+    c_copies = [remote(own_ref, out_ref.at[tp, me], c_send.at[0], c_recv.at[0], {"tp": near})]
+    for k in range(1, n):
+        x_copies.append(along(tp, k, x_send.at[k], x_recv.at[k], {"tp": far}))
+        c_copies.append(along(tp, k, c_send.at[k], c_recv.at[k], {"tp": near}))
+    f_copies = [along(far, k, c_send.at[n + k], c_recv.at[n + k], {"tp": near}) for k in range(n)]
+    x_copies[0].start()
+    for copy in z_copies:
+        copy.start()
+    c_copies[0].start()
+    out_ref[tp, me] = own_ref[...]
+    for k in range(1, n):
+        z_copies[k - 1].wait_recv()
+        x_copies[k].start()
+        c_copies[k].start()
+    for k in range(n):
+        x_copies[k].wait_recv()
+        f_copies[k].start()
+    for copy in c_copies + f_copies:
+        copy.wait_recv()
+    for copy in z_copies + x_copies + c_copies + f_copies:
+        copy.wait_send()
+
+
+def gather_rows(own):
+    n, wide = lax.axis_size("sp"), lax.axis_size("tp")
+    if n > 8 or wide != 4:
+        out = lax.all_gather(own, ("tp", "sp"), axis=0)
+        return out.reshape((wide, n) + own.shape)
+    dma = pltpu.SemaphoreType.DMA
+    return pl.pallas_call(
+        functools.partial(rows_kernel, n),
+        out_shape=jax.ShapeDtypeStruct((wide, n) + own.shape, own.dtype),
+        in_specs=[VMEM],
+        out_specs=VMEM,
+        scratch_shapes=[
+            dma((n - 1,)),
+            dma((n - 1,)),
+            dma((n,)),
+            dma((n,)),
+            dma((2 * n,)),
+            dma((2 * n,)),
+        ],
+        compiler_params=pltpu.CompilerParams(collective_id=2, has_side_effects=True),
+        cost_estimate=pl.CostEstimate(flops=0, bytes_accessed=90_000_000, transcendentals=0),
+        name="gather_rows",
+    )(own)
+
+
+def reduce_kernel(
+    n, chunks, part_ref, base_ref, out_ref, got_c, sum_c, got_x, sum_x, got_z,
+    c_send, c_recv, x_send, x_recv, z_send, z_recv,
+):
+    tp, near, far = partners()
+    low, high = lax.rem(tp, 2), tp // 2
+    shifts = range(1, n)
+    me = lax.axis_index("sp") if n > 1 else 0
+    greet([{"tp": near}, {"tp": far}] + [{"sp": lax.rem(me + k, n)} for k in shifts])
+    width = part_ref.shape[-1] // chunks
+    cols = [pl.ds(i * width, width) for i in range(chunks)]
+    c_copies, x_copies, z_copies = [], [], []
+    for i in range(chunks):
+        copy = remote(
+            part_ref.at[:, 1 - low, :, :, cols[i]],
+            got_c.at[i],
+            c_send.at[i],
+            c_recv.at[i],
+            {"tp": near},
+        )
+        copy.start()
+        c_copies.append(copy)
+    for i in range(chunks):
+        c_copies[i].wait_recv()
+        mine = part_ref[:, low, :, :, cols[i]].astype(jnp.float32)
+        sum_c[i] = (mine + got_c[i].astype(jnp.float32)).astype(sum_c.dtype)
+        copy = remote(
+            sum_c.at[i, 1 - high], got_x.at[i], x_send.at[i], x_recv.at[i], {"tp": far}
+        )
+        copy.start()
+        x_copies.append(copy)
+    for i in range(chunks):
+        x_copies[i].wait_recv()
+        both = sum_c[i, high].astype(jnp.float32) + got_x[i].astype(jnp.float32)
+        sum_x[i] = both.astype(sum_x.dtype)
+        for k in shifts:
+            peer = lax.rem(me + k, n)
+            copy = remote(
+                sum_x.at[i, peer],
+                got_z.at[i, k - 1],
+                z_send.at[i, k - 1],
+                z_recv.at[i, k - 1],
+                {"sp": peer},
+            )
+            copy.start()
+            z_copies.append(copy)
+    for i in range(chunks):
+        total = sum_x[i, me].astype(jnp.float32)
+        for k in shifts:
+            z_copies[i * (n - 1) + k - 1].wait_recv()
+            total = total + got_z[i, k - 1].astype(jnp.float32)
+        out_ref[:, cols[i]] = (base_ref[:, cols[i]] + total).astype(out_ref.dtype)
+    for copy in c_copies + x_copies + z_copies:
+        copy.wait_send()
+
+
+def reduce_rows(part, base, dtype, over_sp):
+    wide, n = part.shape[:2]
+    if n > 8 or wide != 4 or part.size > 8_000_000:
+        axes = ("tp", "sp") if over_sp else "tp"
+        flat = part.reshape(-1, part.shape[-1])
+        total = lax.psum_scatter(flat, axes, scatter_dimension=0, tiled=True)
+        return (base + total.astype(jnp.float32)).astype(dtype)
+    rows, columns = part.shape[2:]
+    chunks = 4 if columns % 512 == 0 else 1
+    width = columns // chunks
+    dma = pltpu.SemaphoreType.DMA
+    zs = max(n - 1, 1)
+    return pl.pallas_call(
+        functools.partial(reduce_kernel, n, chunks),
+        out_shape=jax.ShapeDtypeStruct((rows, columns), dtype),
+        in_specs=[VMEM, VMEM],
+        out_specs=VMEM,
+        scratch_shapes=[
+            pltpu.VMEM((chunks, 2, n, rows, width), part.dtype),
+            pltpu.VMEM((chunks, 2, n, rows, width), part.dtype),
+            pltpu.VMEM((chunks, n, rows, width), part.dtype),
+            pltpu.VMEM((chunks, n, rows, width), part.dtype),
+            pltpu.VMEM((chunks, zs, rows, width), part.dtype),
+            dma((chunks,)),
+            dma((chunks,)),
+            dma((chunks,)),
+            dma((chunks,)),
+            dma((chunks, zs)),
+            dma((chunks, zs)),
+        ],
+        compiler_params=pltpu.CompilerParams(
+            collective_id=3 if over_sp else 4, has_side_effects=True
+        ),
+        cost_estimate=pl.CostEstimate(flops=0, bytes_accessed=60_000_000, transcendentals=0),
+        name="reduce_all" if over_sp else "reduce_tp",
+    )(part.reshape(2, 2, n, rows, columns), base)
 
 
 def rotate(block, positions, heads):
@@ -49,20 +278,23 @@
     if count > 8:
         return lax.all_to_all(pieces, "sp", 0, 0)
     shared = pieces.reshape(count, copies, pieces.shape[1] // copies, *pieces.shape[2:])
-    by_shift = [lax.dynamic_index_in_dim(pieces, me, 0, keepdims=False)]
+    parts = []
     for shift in range(1, count):
         dest = lax.rem(me + shift, count)
         part = lax.dynamic_slice(
             shared, (dest, mine) + (0,) * (shared.ndim - 2), (1, 1) + shared.shape[2:]
         )[0, 0]
-        got = [cyclic(part, "sp", shift)]
-        for turn in range(1, copies):
+        with jax.named_scope("along_sp"):
+            parts.append(cyclic(part, "sp", shift))
+    got = [jnp.stack(parts, axis=0)]
+    for turn in range(1, copies):
+        with jax.named_scope("along_grp"):
             got.append(cyclic(got[0], "grp", turn))
-        got = jnp.stack(got, axis=0)
-        order = [lax.rem(mine - share + copies, copies) for share in range(copies)]
-        got = jnp.stack([lax.dynamic_index_in_dim(got, at, 0, keepdims=False) for at in order])
-        by_shift.append(got.reshape(pieces.shape[1:]))
-    stacked = jnp.stack(by_shift, axis=0)
+    got = jnp.stack(got, axis=0)
+    order = [lax.rem(mine - share + copies, copies) for share in range(copies)]
+    got = jnp.stack([lax.dynamic_index_in_dim(got, at, 0, keepdims=False) for at in order], 1)
+    got = got.reshape((count - 1,) + pieces.shape[1:])
+    stacked = jnp.concatenate([lax.dynamic_index_in_dim(pieces, me, 0), got], axis=0)
     return jnp.stack(
         [
             lax.dynamic_index_in_dim(stacked, lax.rem(me - source + count, count), 0, keepdims=False)
@@ -137,7 +369,7 @@
     packed = jnp.concatenate(
         [k_first, k_second, value, doc_ids.astype(jnp.bfloat16)[..., None]], axis=-1
     )
-    packed = lax.all_gather(packed, "sp", axis=1, tiled=True)
+    packed = gather_sp(packed)
     key_cols = k_first.shape[2]
     keys_one = packed[..., :key_cols]
     keys_two = packed[..., key_cols : 2 * key_cols]
@@ -180,19 +412,18 @@
         seqs * rows, heads * head_width
     )
     heads_out = heads_out.astype(jnp.bfloat16)
-    proj = lax.psum_scatter(
-        jnp.dot(heads_out, out_weight, preferred_element_type=jnp.float32).astype(jnp.bfloat16),
-        "tp",
-        scatter_dimension=0,
-        tiled=True,
-    ).astype(jnp.float32)
-    mid = resid_in.astype(jnp.float32) + proj.reshape(resid_in.shape)
+    own = resid_in.shape[0]
+    features = resid_in.shape[2]
+    proj = jnp.dot(heads_out, out_weight, preferred_element_type=jnp.float32).astype(jnp.bfloat16)
+    mid = reduce_rows(
+        proj.reshape(-1, 1, own * rows, features),
+        resid_in.astype(jnp.float32).reshape(own * rows, features),
+        jnp.float32,
+        False,
+    )
     meansq_mid = jnp.mean(mid * mid, axis=-1, keepdims=True)
     normed = (mid * lax.rsqrt(meansq_mid + NORM_EPS) * norm_gain).astype(jnp.bfloat16)
-    own = normed.shape[0]
-    features = normed.shape[2]
-    gathered = lax.all_gather(normed, ("tp", "sp"), axis=0)
-    gathered = gathered.reshape(-1, n_sp, own, rows, features)
+    gathered = gather_rows(normed).reshape(-1, n_sp, own, rows, features)
     full_rows = jnp.transpose(gathered, (0, 2, 1, 3, 4)).reshape(-1, features)
     total_rows = n_sp * rows
     start = me * share
@@ -208,10 +439,8 @@
     hidden = hidden.reshape(-1, own, n_sp, rows, share)
     hidden = jnp.transpose(hidden, (0, 2, 1, 3, 4)).reshape(-1, share)
     partial_down = jnp.dot(hidden, down_full, preferred_element_type=jnp.float32)
-    down = lax.psum_scatter(
-        partial_down.astype(jnp.bfloat16), ("tp", "sp"), scatter_dimension=0, tiled=True
-    ).astype(jnp.float32)
-    return (mid + down.reshape(mid.shape)).astype(jnp.bfloat16)
+    partial_down = partial_down.astype(jnp.bfloat16).reshape(-1, n_sp, own * rows, features)
+    return reduce_rows(partial_down, mid, jnp.bfloat16, True).reshape(resid_in.shape)
 
 
 def solution(mesh):

time: 292 us -> 260 us (0.89)
  waiting for transfers between devices: 144 us -> 5.69 us
  Pallas kernels: 0 us -> 117 us
  blocking collectives: 21.3 us -> 0 us
  local copies, waits for them, and re-layouts: 40.4 us -> 54.1 us
  between operations: 14.3 us -> 0.99 us
  other arithmetic: 35 us -> 47.8 us
    pallas_call x0 -> x4, Pallas kernels: none -> 117 us  [the longest x2 56.3 us: reduce_rows(): pl.pallas_call(functools.partial(reduce_kernel, n, chunks), out_shape=jax...]
    reduce_scatter x2 -> x0, waiting for transfers between devices: 113 us -> none  [the longest x1 88.7 us: per_device(): lax.psum_scatter(partial_down.astype(jnp.bfloat16), ('tp', 'sp'), scatter...]
    ppermute x12 -> x8, waiting for transfers between devices: 31.4 us -> 5.69 us  [cyclic(): lax.ppermute(array, axis, [(i, (i + by) % length) for i in range(length)])]
    all_gather x1 -> x0, blocking collectives: 21.3 us -> none  [per_device(): packed = lax.all_gather(packed, 'sp', axis=1, tiled=True)]
    unnamed x46 -> x34, local copies, waits for them, and re-layouts: 11.3 us -> 18.6 us
    reshape x4, other arithmetic: 2.85 us -> 6.01 us  [rotate(): entries = block.astype(jnp.float32).reshape(block.shape[:-1] + (heads, -1))]
    another operation x8 -> x4, other arithmetic: 9.15 us -> 7.54 us  [the longest x2 4.66 us: exchange(): got = [jnp.stack(parts, axis=0)]]
    ppermute x12 -> x8, starting transfers between devices: 16.2 us -> 15.1 us  [cyclic(): lax.ppermute(array, axis, [(i, (i + by) % length) for i in range(length)])]
  transfers between devices with their start and end apart: 15 -> 8, of which waited for: 8 -> 1; matrix products, arithmetic and copies ran while one was open for 14% -> 35% of each run, Pallas kernels for 0% -> 28%
where the time goes in v2:
time: 260 us; the launch traced here: 258 us
  Pallas kernels  117 us (45%)
  local copies, waits for them, and re-layouts  54.1 us (21%)
  other arithmetic  47.8 us (18%)
  matrix products  17.1 us (7%)
  starting transfers between devices  15.1 us (6%)
  waiting for transfers between devices  5.69 us (2%)
    pallas_call x2, Pallas kernels, reduce_rows(): pl.pallas_call(functools.partial(reduce_kernel, n, chunks), out_shape=jax...  56.3 us
    pallas_call x1, Pallas kernels, gather_rows(): pl.pallas_call(functools.partial(rows_kernel, n), out_shape=jax.ShapeDtyp...  36.4 us
    pallas_call x1, Pallas kernels, gather_sp(): pl.pallas_call(functools.partial(spread_kernel, n), out_shape=jax.ShapeDt...  24.6 us
    unnamed x34, local copies, waits for them, and re-layouts  18.6 us
    ppermute x8, starting transfers between devices, cyclic(): lax.ppermute(array, axis, [(i, (i + by) % length) for i in range(length)])  15.1 us
    reshape x1, local copies, waits for them, and re-layouts, exchange(): pieces.reshape(count, copies, pieces.shape[1] // copies, *pieces.shape[2:])  6.92 us
    reshape x4, other arithmetic, rotate(): entries = block.astype(jnp.float32).reshape(block.shape[:-1] + (heads, -1))  6.01 us
    convert_element_type x1, other arithmetic, per_device(): hidden = (jax.nn.silu(conv_g) * conv_v).astype(jnp.bfloat16)  5.94 us
  transfers between devices with their start and end apart: 8, of which 1 were waited for; matrix products, arithmetic and copies ran while one was open for 35% of the time, Pallas kernels for 28%

profile of v2, /device:TPU:0, one launch (start us, length us, event | category | flops | bytes accessed | tf_op | source)
XLA Modules:
  0.0 258.0 jit_solution(743260196842443101)
XLA Ops:
  0.0 2.1 dynamic-slice_bitcast_fusion.2
  2.1 3.1 %collective-permute-start.4 = (bf16[176,512]{1,0:T(8,128)(2,1)}, bf16[176,512]{1,0:T(8,128)(2,1)}, u32[]{:S(2)}, u32[]{:S(2)}) collective-permute-start(bf16[176,512]{1,0:T(8,128)(2,1)} %get-tuple-element.133), channel_id=1, source_target_pairs={{0,4},{4,8},{8,12},{12,0},{1,5},{5,9},{9,13},{13,1},{2,6},{6,10},{... | collective-permute-start | bytes 540680 | tf_op jit(solution)/shard_map/along_sp/ppermute | solution.py:270
  5.1 2.6 %collective-permute-start.5 = (bf16[176,512]{1,0:T(8,128)(2,1)}, bf16[176,512]{1,0:T(8,128)(2,1)}, u32[]{:S(2)}, u32[]{:S(2)}) collective-permute-start(bf16[176,512]{1,0:T(8,128)(2,1)} %get-tuple-element.135), channel_id=1, source_target_pairs={{0,8},{4,12},{8,0},{12,4},{1,9},{5,13},{9,1},{13,5},{2,10},{6,14},... | collective-permute-start | bytes 540680 | tf_op jit(solution)/shard_map/along_sp/ppermute | solution.py:270
  9.4 2.5 copy.52
  12.0 3.2 %fusion.26 = bf16[4,512,2,352]{1,3,0,2:T(8,128)(2,1)} fusion(bf16[512,1,4,352]{0,3,2,1:T(8,128)(2,1)} %bitcast.161, bf16[512,1,4,352]{0,3,2,1:T(8,128)(2,1)S(1)} %bitcast.159), kind=kLoop, calls=%fused_computation.48 | loop fusion | flops 1441792 | bytes 5767168 | tf_op jit(solution)/shard_map/transpose | solution.py:347
  15.2 6.9 %reshape.253 = bf16[4,2,256,2,352]{2,1,4,0,3:T(2,128)(2,1)} reshape(bf16[4,512,2,352]{1,3,0,2:T(8,128)(2,1)} %fusion.26) | data formatting | bytes 5767168 | tf_op jit(solution)/shard_map/reshape | solution.py:280
  22.1 3.8 %constant_dynamic-slice_fusion.4 = (bf16[1,1,256,2,352]{2,1,4,0,3:T(2,128)(2,1)S(1)}, bf16[1,1,256,2,352]{2,1,4,0,3:T(2,128)(2,1)S(1)}, bf16[1,1,256,2,352]{2,1,4,0,3:T(2,128)(2,1)S(1)}) fusion(bf16[4,2,256,2,352]{2,1,4,0,3:T(2,128)(2,1)} %reshape.253, s32[]{:T(128)S(6)} %select_n.89, s32[]{:T(128)S(6)} %select_n.90, s32[]{:T(128)S(6)} %select_n.91, ...), kind=kLoop, calls=%fused_computation.150 | loop fusion | bytes 2162704 | tf_op jit(solution)/shard_map/dynamic_slice | solution.py:284
  27.5 1.9 collective-permute-start.1
  30.2 1.9 collective-permute-start.2
  50.6 24.6 %gather_sp.1 = bf16[4,4,64,257]{3,2,1,0:T(8,128)(2,1)} custom-call(bf16[4,64,257]{2,1,0:T(8,128)(2,1)} %pad_maximum_fusion.6.own_ref), custom_call_target="tpu_custom_call" | custom-call | bytes 30000000 | tf_op jit(solution)/shard_map/gather_sp/pallas_call | solution.py:66
  79.8 1.7 copy.47
  81.5 1.8 convert.47
  85.1 1.8 convert.48
  92.9 12.4 %conditional.1 = (f32[4,2,4,64]{3,2,1,0:T(4,128)S(1)}, f32[4,2,4,64,64]{4,3,2,1,0:T(8,128)}, f32[4,2,4,64]{3,2,1,0:T(4,128)}, f32[4,2,4,64,64]{4,3,2,1,0:T(8,128)}) conditional(s32[]{:T(128)} %bitcast.13, () %tuple.15, (s32[64]{0:T(128)}, s32[4,256]{1,0:T(4,128)}, s32[4,64]{1,0:T(4,128)}, bf16[4,256,257]{2,1,0:T(8,128)(2,1)}, ...), branch_computations={%region_0.1_spmd, %region_1.6_spmd} | conditional | flops 215379968 | bytes 19970448 | solution.py:404
  92.9 2.3 copy.49
  105.3 2.3 multiply_reduce_fusion
  109.3 2.1 convert_element_type.107
  111.3 1.8 bitcast_convert_fusion.base_ref
  113.1 2.7 %convolution_convert_fusion.1 = bf16[256,2048]{1,0:T(8,128)(2,1)} fusion(bf16[256,512]{1,0:T(8,128)(2,1)} %convert_element_type.107, bf16[512,2048]{1,0:T(8,128)(2,1)S(1)} %copy-done), kind=kOutput, calls=%fused_computation.50 | convolution fusion | flops 537395200 | bytes 3407872 | tf_op jit(solution)/shard_map/dot_general | solution.py:417
  115.8 12.4 %reduce_tp.1.base_ref = f32[64,2048]{1,0:T(8,128)} custom-call(bf16[2,2,1,64,2048]{4,3,2,1,0:T(8,128)(2,1)} %bitcast.170, f32[64,2048]{1,0:T(8,128)} %bitcast_convert_fusion.base_ref), custom_call_target="tpu_custom_call" | custom-call | bytes 60000000 | tf_op jit(solution)/shard_map/reduce_tp/pallas_call | solution.py:216
  129.4 3.6 %collective-permute-start.6 = (bf16[176,512]{1,0:T(8,128)(2,1)S(1)}, bf16[176,512]{1,0:T(8,128)(2,1)S(1)}, u32[]{:S(2)}, u32[]{:S(2)}) collective-permute-start(bf16[176,512]{1,0:T(8,128)(2,1)S(1)} %copy-done.8), channel_id=1, source_target_pairs={{0,12},{4,0},{8,4},{12,8},{1,13},{5,1},{9,5},{13,9},{2,14},{6,2},{... | collective-permute-start | bytes 540680 | tf_op jit(solution)/shard_map/along_sp/ppermute | solution.py:270
  133.0 5.7 %collective-permute-done.6 = bf16[176,512]{1,0:T(8,128)(2,1)S(1)} collective-permute-done((bf16[176,512]{1,0:T(8,128)(2,1)S(1)}, bf16[176,512]{1,0:T(8,128)(2,1)S(1)}, u32[]{:S(2)}, u32[]{:S(2)}) %collective-permute-start.6) | collective-permute-done | bytes 180256 | tf_op jit(solution)/shard_map/along_sp/ppermute | solution.py:270
  138.7 2.0 pad_maximum_fusion.3
  142.2 2.7 %pad_maximum_fusion.1 = (bf16[3,256,2,352]{1,3,2,0:T(8,128)(2,1)}, bf16[1,3,256,2,352]{2,4,3,1,0:T(8,128)(2,1)}) fusion(bf16[1,256,2,352]{1,3,2,0:T(8,128)(2,1)} %bitcast.44, bf16[1,256,2,352]{1,3,2,0:T(8,128)(2,1)} %bitcast.42, bf16[1,256,2,352]{1,3,2,0:T(8,128)(2,1)} %bitcast.40), kind=kLoop, calls=%fused_computation.100 | loop fusion | flops 1081344 | bytes 3244032 | tf_op jit(solution)/shard_map/stack | solution.py:289
  146.2 36.4 %gather_rows.1 = bf16[4,4,64,2048]{3,2,1,0:T(8,128)(2,1)} custom-call(bf16[64,2048]{1,0:T(8,128)(2,1)} %multiply_convert_fusion.1.own_ref), custom_call_target="tpu_custom_call" | custom-call | bytes 90000000 | tf_op jit(solution)/shard_map/gather_rows/pallas_call | solution.py:129
  188.6 2.0 fusion.50
  193.1 1.8 copy-done.5
  196.6 2.8 %fusion.46 = f32[1024,352]{0,1:T(8,128)} fusion(bf16[1024,2048]{1,0:T(8,128)(2,1)S(1)} %bitcast.169, bf16[2048,2,352]{0,2,1:T(8,128)(2,1)S(1)} %bitcast.172), kind=kOutput, calls=%fused_computation.91 | convolution fusion | flops 1477115904 | bytes 7077888 | tf_op jit(solution)/shard_map/dot_general | solution.py:433
  200.1 1.9 reshape.273
  202.0 5.9 %fusion.42 = bf16[4,256,352]{1,0,2:T(4,128)(2,1)S(1)} fusion(f32[4,256,352]{1,0,2:T(4,128)S(1)} %reshape.273, f32[4,256,352]{1,0,2:T(4,128)S(1)} %reshape.272, f32[352]{0:T(512)S(1)} %get-tuple-element.108, f32[352]{0:T(512)S(1)} %get-tuple-element.107, f32[352]{0:T(512)S(1)} %get-tuple-element.106, f32[352]{0:T(512)S(1)} %get-tuple-element.160, ...), kind=kLoop, calls=%fused_computation.87 | loop fusion | flops 7208960 | bytes 3614976 | tf_op jit(solution)/shard_map/convert_element_type | solution.py:438
  208.1 4.3 %convolution_convert_fusion = bf16[1024,2048]{1,0:T(8,128)(2,1)} fusion(bf16[1024,352]{0,1:T(8,128)(2,1)S(1)} %bitcast.178, bf16[352,2048]{1,0:T(8,128)(2,1)S(1)} %bitcast.174), kind=kOutput, calls=%fused_computation.40 | convolution fusion | flops 1478492160 | bytes 6356992 | tf_op jit(solution)/shard_map/dot_general | solution.py:441
  212.4 43.9 %reduce_all.1 = bf16[64,2048]{1,0:T(8,128)(2,1)} custom-call(bf16[2,2,4,64,2048]{4,3,2,1,0:T(8,128)(2,1)} %bitcast.167, f32[64,2048]{1,0:T(8,128)} %reduce_tp.1.base_ref), custom_call_target="tpu_custom_call" | custom-call | bytes 60000000 | tf_op jit(solution)/shard_map/reduce_all/pallas_call | solution.py:216
  (103 shorter events, 62.5 us)
Async XLA Ops:
  0.0 113.1 %copy-start = (bf16[512,2048]{1,0:T(8,128)(2,1)S(1)}, bf16[512,2048]{1,0:T(8,128)(2,1)}, u32[]{:S(2)}) copy-start(bf16[512,2048]{1,0:T(8,128)(2,1)} %param.27) | copy-start | bytes 6291460
  2.1 127.3 %collective-permute-start.4 = (bf16[176,512]{1,0:T(8,128)(2,1)}, bf16[176,512]{1,0:T(8,128)(2,1)}, u32[]{:S(2)}, u32[]{:S(2)}) collective-permute-start(bf16[176,512]{1,0:T(8,128)(2,1)} %get-tuple-element.133), channel_id=1, source_target_pairs={{0,4},{4,8},{8,12},{12,0},{1,5},{5,9},{9,13},{13,1},{2,6},{6,10},{... | collective-permute-start | bytes 540680 | tf_op jit(solution)/shard_map/along_sp/ppermute | solution.py:270
  5.1 127.9 %collective-permute-start.5 = (bf16[176,512]{1,0:T(8,128)(2,1)}, bf16[176,512]{1,0:T(8,128)(2,1)}, u32[]{:S(2)}, u32[]{:S(2)}) collective-permute-start(bf16[176,512]{1,0:T(8,128)(2,1)} %get-tuple-element.135), channel_id=1, source_target_pairs={{0,8},{4,12},{8,0},{12,4},{1,9},{5,13},{9,1},{13,5},{2,10},{6,14},... | collective-permute-start | bytes 540680 | tf_op jit(solution)/shard_map/along_sp/ppermute | solution.py:270
  26.7 115.5 %collective-permute-start = (bf16[256,2,352]{0,2,1:T(8,128)(2,1)}, bf16[256,2,352]{0,2,1:T(8,128)(2,1)}, u32[]{:S(2)}, u32[]{:S(2)}) collective-permute-start(bf16[256,2,352]{0,2,1:T(8,128)(2,1)} %bitcast.158), channel_id=1, source_target_pairs={{0,4},{4,8},{8,12},{12,0},{1,5},{5,9},{9,13},{13,1},{2,6},{6,10},{... | collective-permute-start | bytes 1081352 | tf_op jit(solution)/shard_map/along_sp/ppermute | solution.py:270
  27.5 114.7 %collective-permute-start.1 = (bf16[256,2,352]{0,2,1:T(8,128)(2,1)}, bf16[256,2,352]{0,2,1:T(8,128)(2,1)}, u32[]{:S(2)}, u32[]{:S(2)}) collective-permute-start(bf16[256,2,352]{0,2,1:T(8,128)(2,1)} %bitcast.157), channel_id=1, source_target_pairs={{0,8},{4,12},{8,0},{12,4},{1,9},{5,13},{9,1},{13,5},{2,10},{6,14},... | collective-permute-start | bytes 1081352 | tf_op jit(solution)/shard_map/along_sp/ppermute | solution.py:270
  30.2 112.0 %collective-permute-start.2 = (bf16[256,2,352]{0,2,1:T(8,128)(2,1)}, bf16[256,2,352]{0,2,1:T(8,128)(2,1)}, u32[]{:S(2)}, u32[]{:S(2)}) collective-permute-start(bf16[256,2,352]{0,2,1:T(8,128)(2,1)} %bitcast.156), channel_id=1, source_target_pairs={{0,12},{4,0},{8,4},{12,8},{1,13},{5,1},{9,5},{13,9},{2,14},{6,2},{... | collective-permute-start | bytes 1081352 | tf_op jit(solution)/shard_map/along_sp/ppermute | solution.py:270
  92.9 4.7 %copy-start.14 = (s32[64]{0:T(128)S(1)}, s32[64]{0:T(128)}, u32[]{:S(2)}) copy-start(s32[64]{0:T(128)} %get-tuple-element.42) | copy-start | bytes 772 | tf_op jit(solution)/shard_map/cond
  92.9 4.8 %copy-start.10 = (s32[4,256]{1,0:T(4,128)S(1)}, s32[4,256]{1,0:T(4,128)}, u32[]{:S(2)}) copy-start(s32[4,256]{1,0:T(4,128)} %get-tuple-element.43) | copy-start | bytes 12292 | tf_op jit(solution)/shard_map/cond
  92.9 4.8 %copy-start.12 = (s32[4,64]{1,0:T(4,128)S(1)}, s32[4,64]{1,0:T(4,128)}, u32[]{:S(2)}) copy-start(s32[4,64]{1,0:T(4,128)} %get-tuple-element.44) | copy-start | bytes 3076 | tf_op jit(solution)/shard_map/cond
  95.2 2.7 %copy-start.7 = (bf16[4,64,2,4,32]{1,4,3,2,0:T(8,128)(2,1)S(1)}, bf16[4,64,2,4,32]{1,4,3,2,0:T(8,128)(2,1)}, u32[]{:S(2)}) copy-start(bf16[4,64,2,4,32]{1,4,3,2,0:T(8,128)(2,1)} %get-tuple-element.47) | copy-start | bytes 393220 | tf_op jit(solution)/shard_map/cond
  105.3 2.4 copy-start.13
  115.8 13.6 %copy-start.8 = (bf16[176,512]{1,0:T(8,128)(2,1)S(1)}, bf16[176,512]{1,0:T(8,128)(2,1)}, u32[]{:S(2)}) copy-start(bf16[176,512]{1,0:T(8,128)(2,1)} %get-tuple-element.134) | copy-start | bytes 540676
  129.4 9.3 %collective-permute-start.6 = (bf16[176,512]{1,0:T(8,128)(2,1)S(1)}, bf16[176,512]{1,0:T(8,128)(2,1)S(1)}, u32[]{:S(2)}, u32[]{:S(2)}) collective-permute-start(bf16[176,512]{1,0:T(8,128)(2,1)S(1)} %copy-done.8), channel_id=1, source_target_pairs={{0,12},{4,0},{8,4},{12,8},{1,13},{5,1},{9,5},{13,9},{2,14},{6,2},{... | collective-permute-start | bytes 540680 | tf_op jit(solution)/shard_map/along_sp/ppermute | solution.py:270
  138.7 6.7 %copy-start.3 = (f32[64,2048]{1,0:T(8,128)S(1)}, f32[64,2048]{1,0:T(8,128)}, u32[]{:S(2)}) copy-start(f32[64,2048]{1,0:T(8,128)} %reduce_tp.1.base_ref) | copy-start | bytes 1572868
  138.7 6.7 %copy-start.11 = (f32[2048]{0:T(1024)S(1)}, f32[2048]{0:T(1024)}, u32[]{:S(2)}) copy-start(f32[2048]{0:T(1024)} %param.28) | copy-start | bytes 24580
  140.6 44.2 %collective-permute-start.7 = (bf16[3,176,512]{2,1,0:T(8,128)(2,1)}, bf16[3,176,512]{2,1,0:T(8,128)(2,1)}, u32[]{:S(2)}, u32[]{:S(2)}) collective-permute-start(bf16[3,176,512]{2,1,0:T(8,128)(2,1)} %get-tuple-element.140), channel_id=1, source_target_pairs={{0,16},{16,0},{1,17},{17,1},{2,18},{18,2},{3,19},{19,3},{4,20},{20... | collective-permute-start | bytes 1622024 | tf_op jit(solution)/shard_map/along_grp/ppermute | solution.py:270
  144.9 43.6 %collective-permute-start.3 = (bf16[3,256,2,352]{1,3,2,0:T(8,128)(2,1)}, bf16[3,256,2,352]{1,3,2,0:T(8,128)(2,1)}, u32[]{:S(2)}, u32[]{:S(2)}) collective-permute-start(bf16[3,256,2,352]{1,3,2,0:T(8,128)(2,1)} %get-tuple-element.138), channel_id=1, source_target_pairs={{0,16},{16,0},{1,17},{17,1},{2,18},{18,2},{3,19},{19,3},{4,20},{20... | collective-permute-start | bytes 3244040 | tf_op jit(solution)/shard_map/along_grp/ppermute | solution.py:270
  146.2 38.4 %copy-start.2 = (bf16[512,1408]{0,1:T(8,128)(2,1)S(1)}, bf16[512,1408]{0,1:T(8,128)(2,1)}, u32[]{:S(2)}) copy-start(bf16[512,1408]{0,1:T(8,128)(2,1)} %copy.52) | copy-start | bytes 4325380
  183.6 1.1 copy-start.9
  187.1 1.5 copy-start.4
  192.7 2.2 copy-start.5
  202.0 6.1 %copy-start.6 = (bf16[4,44,8,512]{3,2,0,1:T(8,128)(2,1)S(1)}, bf16[4,44,8,512]{3,2,0,1:T(8,128)(2,1)}, u32[]{:S(2)}) copy-start(bf16[4,44,8,512]{3,2,0,1:T(8,128)(2,1)} %copy.68) | copy-start | bytes 4325380
  212.4 45.6 %copy-start.1 = (bf16[512,2048]{1,0:T(8,128)(2,1)S(1)}, bf16[512,2048]{1,0:T(8,128)(2,1)}, u32[]{:S(2)}) copy-start(bf16[512,2048]{1,0:T(8,128)(2,1)} %param.27) | copy-start | bytes 6291460
